TPU v7x, 256 devices: a whole 4x4x8 slice. The times are simulated.
256 devices in a mesh: sp: 64 (over z, x, core), tp: 4 (over y).
Axes of the slice: x: 4, y: 4, z: 8, core: 2. Of those that a mesh axis runs over, the one named last changes fastest.
Arguments:
- residual_in: bfloat16 [32768, 2048], P('sp'), may hold values from -6 to 6
- gate_in: bfloat16 [32768, 2048], P('sp', 'tp'), may hold values from -6 to 6
- value_in: bfloat16 [32768, 2048], P('sp', 'tp'), may hold values from -6 to 6
- conv_weight: float32 [4, 2048], P(None, 'tp'), may hold values from -3 to 3
- rate_weight: bfloat16 [32, 64, 64], P('tp'), may hold values from -0.75 to 0.75
- input_weight: bfloat16 [32, 64, 64], P('tp'), may hold values from -0.75 to 0.75
- decay_base: float32 [2048], P('tp'), may hold values from 3.8146973e-07 to 0.015, as said below
- step_scale: float32 [32768, 2048], P('sp', 'tp'), may hold values from 0.25 to 458752, as said below
- out_weight: bfloat16 [2048, 2048], P('tp'), may hold values from -0.375 to 0.375
- norm_gain: float32 [2048], replicated, may hold values from 0.1 to 1.9
- up_weight: bfloat16 [2048, 8192], P('sp', 'tp'), may hold values from -0.125 to 0.125
- down_weight: bfloat16 [2048, 8192], P('sp', 'tp'), may hold values from -0.0625 to 0.0625
Outputs:
- block_out: bfloat16 [32768, 2048], P(('sp', 'tp'))
Inputs may be any that keep to these rules, and one draw needn't show every extreme that they name: `decay_base`: positive. `step_scale`: positive.
All inputs are finite; a program needn't handle non-finite values.
Results may differ from a plain program's by a relative error of at most 0.018.
Values may be sent and summed in bfloat16 or wider, within the bound.
A program may use at most 128 MiB of HBM per device.

v0:
```python
import math

import jax
import jax.numpy as jnp
from jax import lax
from jax.sharding import Mesh
from jax.sharding import PartitionSpec as P

SP = ("sp_0", "sp_1", "sp_2")
SP_TP = ("sp_0", "sp_1", "sp_2", "tp")


def sent_together(arrays, axis, dim, along):
    widths = [a.shape[along] for a in arrays]
    both = jnp.concatenate(arrays, axis=along)
    filled = lax.all_gather(both, axis, axis=dim, tiled=True)
    return tuple(jnp.split(filled, [sum(widths[:k]) for k in range(1, len(widths))], axis=along))


def shifted(block, axis, distance):
    devices = range(lax.axis_size(axis))
    route = [(i - distance, i) for i in devices if i - distance in devices]
    return lax.ppermute(block, axis, route)


def nothing_yet(value, identity):
    return jax.tree.map(
        lambda part, zero: jnp.zeros_like(part) + jnp.asarray(zero, part.dtype), value, identity
    )


def gathered_once(value, axis):
    leaves = jax.tree.leaves(value)
    turns = sorted(range(len(leaves)), key=lambda k: -leaves[k].size)
    width = (1, *leaves[turns[0]].shape)[-1]
    lines = [
        jnp.pad(leaves[k].reshape(-1), (0, -leaves[k].size % width)).reshape(-1, width)
        for k in turns
    ]
    both, at, found = (lax.all_gather(jnp.concatenate(lines), axis), 0, {})
    for k, line in zip(turns, lines):
        section = both[:, at : at + len(line)].reshape(len(both), -1)
        found[k] = section[:, : leaves[k].size].reshape(-1, *leaves[k].shape)
        at += len(line)
    numbers = iter(range(len(leaves)))
    return jax.tree.map(lambda _: found[next(numbers)], value)


def prefix_by_axis(value, axes, combine, identity):
    before = start = nothing_yet(value, identity)
    subtotal = value
    for axis in reversed(axes):
        size, index = (lax.axis_size(axis), lax.axis_index(axis))
        pieces = gathered_once(subtotal, axis)
        inside, subtotal = (start, start)
        for k in range(size):
            passed = k < index
            subtotal = combine(subtotal, jax.tree.map(lambda part: part[k], pieces))
            inside = jax.tree.map(lambda new, old: jnp.where(passed, new, old), subtotal, inside)
        before = combine(inside, before)
    return before


def split_up(value, dim, size):
    before, after = (value.shape[:dim], value.shape[dim + 1 :])
    return jnp.moveaxis(value.reshape(*before, size, -1, *after), dim, 0)


def sum_at_owner(value, axis, dim):
    size = lax.axis_size(axis)
    pieces = lax.all_to_all(split_up(value, dim, size), axis, 0, 0, tiled=True)
    return jnp.sum(pieces.astype(jnp.float32), axis=0)


def copy_for_each(value, axis):
    copies = jnp.broadcast_to(value, (lax.axis_size(axis), *value.shape))
    return lax.all_to_all(copies, axis, split_axis=0, concat_axis=0, tiled=True)


def laid_out(pieces, dim):
    dims = list(pieces.shape[1:])
    dims[dim] *= pieces.shape[0]
    return jnp.moveaxis(pieces, 0, dim).reshape(dims)


def gathered_copies(value, axis, dim):
    pieces = copy_for_each(value, axis)
    return laid_out(pieces, dim)


def chain_join(earlier, later):
    return (earlier[0] * later[0], later[0] * earlier[1] + later[1])


def rounded(term):
    return lax.optimization_barrier(term.astype(jnp.bfloat16)).astype(jnp.float32)


def settle_rows(rows_in, norm_gain):
    widened = rows_in.astype(jnp.float32)
    factor = lax.rsqrt(jnp.mean(widened * widened, axis=-1, keepdims=True) + 1e-06)
    return (widened * factor * norm_gain).astype(jnp.bfloat16)


def step_rows(carry, inputs):
    keep_row, drive_row = inputs
    new_product = carry[0] * keep_row
    new_state = keep_row * carry[1] + drive_row
    return ((new_product, new_state), (new_product, new_state))


def local(
    residual_in,
    gate_in,
    value_in,
    conv_weight,
    rate_weight,
    input_weight,
    decay_base,
    step_scale,
    out_weight,
    norm_gain,
    up_weight,
    down_weight,
):
    row_count = value_in.shape[0]
    tap_count = conv_weight.shape[0]
    channel_count = value_in.shape[1]
    whole_up, whole_down = sent_together((up_weight, down_weight), SP, 0, 1)
    earlier_rows = shifted(value_in[row_count - tap_count + 1 :], SP, 1)
    padded = jnp.concatenate([earlier_rows, value_in], axis=0).astype(jnp.float32)
    filtered_rows = jnp.zeros(value_in.shape, jnp.float32)
    for offset in range(tap_count):
        filtered_rows = filtered_rows + padded[offset : offset + row_count] * conv_weight[offset]
    smoothed = filtered_rows.astype(jnp.bfloat16)
    grouped = smoothed.reshape(row_count, rate_weight.shape[0], rate_weight.shape[1])
    rate_gate = jax.nn.sigmoid(
        jnp.einsum("tnd,nde->tne", grouped, rate_weight, preferred_element_type=jnp.float32)
    ).reshape(row_count, -1)
    input_gate = jax.nn.sigmoid(
        jnp.einsum("tnd,nde->tne", grouped, input_weight, preferred_element_type=jnp.float32)
    ).reshape(row_count, -1)
    log_keep = -8.0 * step_scale * rate_gate * decay_base[None, :]
    drive = jnp.sqrt(-jnp.expm1(2.0 * log_keep)) * input_gate * smoothed.astype(jnp.float32)
    block_rows = math.gcd(row_count, 16)
    block_count = row_count // block_rows
    keep_blocks = (
        jnp.exp(log_keep).reshape(block_count, block_rows, channel_count).transpose(1, 0, 2)
    )
    drive_blocks = drive.reshape(block_count, block_rows, channel_count).transpose(1, 0, 2)
    start_carry = (
        jnp.ones((block_count, channel_count), jnp.float32),
        jnp.zeros((block_count, channel_count), jnp.float32),
    )
    final_carry, inner = lax.scan(step_rows, start_carry, (keep_blocks, drive_blocks))
    inner_products, inner_states = inner
    prefix_products, prefix_states = lax.associative_scan(chain_join, final_carry, axis=0)
    carried = prefix_by_axis(
        (prefix_products[-1], prefix_states[-1]),
        SP,
        chain_join,
        (jnp.ones_like(prefix_products[-1]), jnp.zeros_like(prefix_states[-1])),
    )
    entry_products = jnp.concatenate(
        [jnp.ones((1, channel_count), jnp.float32), prefix_products[:-1]], axis=0
    )
    entry_states = jnp.concatenate(
        [jnp.zeros((1, channel_count), jnp.float32), prefix_states[:-1]], axis=0
    )
    entering = entry_states + entry_products * carried[1][None, :]
    carry_state = (
        (inner_states + inner_products * entering[None, :, :])
        .transpose(1, 0, 2)
        .reshape(row_count, channel_count)
    )
    gated = (jax.nn.gelu(gate_in.astype(jnp.float32), approximate=True) * carry_state).astype(
        jnp.bfloat16
    )
    group_rows = row_count // lax.axis_size("tp")
    own_start = lax.axis_index("tp") * group_rows
    mixed = sum_at_owner(
        rounded(jnp.dot(gated, out_weight, preferred_element_type=jnp.float32)).astype(
            jnp.bfloat16
        ),
        "tp",
        0,
    )
    own_residual = lax.dynamic_slice_in_dim(residual_in, own_start, group_rows, 0)
    own_updated = (own_residual.astype(jnp.float32) + mixed).astype(jnp.bfloat16)
    normed = gathered_copies(settle_rows(own_updated, norm_gain), "tp", 0)
    lifted = jnp.dot(normed, whole_up, preferred_element_type=jnp.float32)
    activated = jnp.square(jax.nn.relu(lifted)).astype(jnp.bfloat16)
    partial_rows = lax.dot_general(
        activated, whole_down, (((1,), (1,)), ((), ())), preferred_element_type=jnp.float32
    )
    summed = sum_at_owner(rounded(partial_rows).astype(jnp.bfloat16), "tp", 0)
    return (own_updated.astype(jnp.float32) + summed).astype(jnp.bfloat16)


def solution(mesh):
    split = Mesh(mesh.devices.reshape(8, 4, 2, mesh.shape["tp"]), ("sp_0", "sp_1", "sp_2", "tp"))
    return jax.shard_map(
        local,
        mesh=split,
        in_specs=(
            P(SP, None),
            P(SP, "tp"),
            P(SP, "tp"),
            P(None, "tp"),
            P("tp", None, None),
            P("tp", None, None),
            P("tp"),
            P(SP, "tp"),
            P("tp", None),
            P(),
            P(SP, "tp"),
            P(SP, "tp"),
        ),
        out_specs=P(SP_TP, None),
        check_vma=False,
    )
```

profile of v0, /device:TPU:64, one launch (start us, length us, event | category | flops | bytes accessed | tf_op | source)
XLA Modules:
  0.0 263.8 jit_solution(1753119246335385714)
XLA Ops:
  6.5 1.8 pad_maximum_fusion
  9.3 1.9 collective-permute-start
  12.1 2.0 copy.32
  14.1 1.6 copy.30
  15.7 2.0 collective-permute-done
  17.7 1.4 maximum_convert_fusion
  22.0 2.7 %fusion.33 = (f32[512,512]{0,1:T(8,128)}, f32[512,512]{0,1:T(8,128)}) fusion(f32[8,512,64]{1,2,0:T(8,128)S(1)} %fusion.14, f32[512]{0:T(512)S(1)} %copy-done.5, f32[8,512,64]{1,2,0:T(8,128)S(1)} %fusion.17, f32[512,512]{0,1:T(8,128)S(1)} %copy.30, f32[512]{0:T(512)S(1)} %bitcast.149, f32[515,512]{0,1:T(8,128)S(1)} %maximum_convert_fusion, ...), kind=kLoop, calls=%fused_computation.51 | loop fusion | flops 4194304 | bytes 9447424 | tf_op jit(solution)/shard_map/mul | solution.py:144
  24.6 2.7 %copy.36 = f32[512,512]{1,0:T(8,128)} copy(f32[512,512]{0,1:T(8,128)} %get-tuple-element.109) | data formatting | bytes 2097152 | tf_op jit(solution)/shard_map/mul | solution.py:144
  28.6 93.1 %while.17 = (s32[]{:T(128)}, f32[32,512]{1,0:T(8,128)S(1)}, f32[32,512]{1,0:T(8,128)S(1)}, f32[16,32,512]{2,0,1:T(8,128)}, f32[16,32,512]{2,0,1:T(8,128)}, /*ind...) while((s32[]{:T(128)}, f32[32,512]{1,0:T(8,128)S(1)}, ...), condition=%wide.region_1.2_spmd.clone, body=%wide.region_0.1_spmd.clone.sunk | while | flops 81923 | bytes 1179763 | solution.py:155
  28.6 1.3 constant_dynamic-slice_fusion.3
  30.0 2.1 dynamic_update_slice.12
  32.2 2.1 dynamic_update_slice.11
  34.4 1.3 constant_dynamic-slice_fusion.3
  35.8 2.1 dynamic_update_slice.12
  38.0 2.1 dynamic_update_slice.11
  40.1 1.3 constant_dynamic-slice_fusion.3
  41.6 2.1 dynamic_update_slice.12
  43.8 2.1 dynamic_update_slice.11
  45.9 1.3 constant_dynamic-slice_fusion.3
  47.4 2.1 dynamic_update_slice.12
  49.6 2.1 dynamic_update_slice.11
  53.2 2.1 dynamic_update_slice.12
  55.4 2.1 dynamic_update_slice.11
  58.9 2.1 dynamic_update_slice.12
  61.1 2.1 dynamic_update_slice.11
  63.2 1.5 constant_dynamic-slice_fusion.3
  64.8 2.1 dynamic_update_slice.12
  67.0 2.1 dynamic_update_slice.11
  69.1 1.3 constant_dynamic-slice_fusion.3
  70.6 2.1 dynamic_update_slice.12
  72.8 2.1 dynamic_update_slice.11
  75.0 1.5 constant_dynamic-slice_fusion.3
  76.6 2.1 dynamic_update_slice.12
  78.8 2.1 dynamic_update_slice.11
  81.0 1.3 constant_dynamic-slice_fusion.3
  82.4 2.1 dynamic_update_slice.12
  84.6 2.1 dynamic_update_slice.11
  86.8 1.4 constant_dynamic-slice_fusion.3
  88.2 2.1 dynamic_update_slice.12
  90.5 2.1 dynamic_update_slice.11
  92.6 1.3 constant_dynamic-slice_fusion.3
  94.1 2.1 dynamic_update_slice.12
  96.3 2.1 dynamic_update_slice.11
  98.4 1.3 constant_dynamic-slice_fusion.3
  99.9 2.1 dynamic_update_slice.12
  102.1 2.1 dynamic_update_slice.11
  104.3 1.3 constant_dynamic-slice_fusion.3
  105.7 2.2 dynamic_update_slice.12
  108.0 2.1 dynamic_update_slice.11
  111.6 2.1 dynamic_update_slice.12
  113.8 2.1 dynamic_update_slice.11
  117.4 2.1 dynamic_update_slice.12
  119.6 2.1 dynamic_update_slice.11
  126.9 1.9 all-gather.3
  128.9 12.0 %all-gather.4 = f32[4,2,512]{2,1,0:T(2,128)S(1)} all-gather(f32[1,2,512]{2,1,0:T(2,128)S(1)} %maximum_bitcast_fusion.1), channel_id=3, replica_groups=mesh['sp_0'=8,'sp_1'=4,'sp_2'=2,'tp'=4] {'sp_1'}, dimensions={0}, use_global_device_ids=true | all-gather | bytes 20480 | tf_op jit(solution)/shard_map/all_gather | solution.py:40
  140.9 27.6 %all-gather.5 = f32[8,2,512]{2,1,0:T(2,128)S(1)} all-gather(f32[1,2,512]{2,1,0:T(2,128)S(1)} %maximum_bitcast_fusion.2), channel_id=4, replica_groups=mesh['sp_0'=8,'sp_1'=4,'sp_2'=2,'tp'=4] {'sp_0'}, dimensions={0}, use_global_device_ids=true | all-gather | bytes 36864 | tf_op jit(solution)/shard_map/all_gather | solution.py:40
  168.7 1.5 multiply_add_fusion
  170.6 2.6 convolution_convert_fusion
  173.2 4.5 %all-to-all-start = ((bf16[4,128,2048]{2,1,0:T(8,128)(2,1)}), bf16[4,128,2048]{2,1,0:T(8,128)(2,1)}, u32[]{:S(2)}, u32[]{:S(2)}) async-start(bf16[4,128,2048]{2,1,0:T(8,128)(2,1)} %bitcast.137), calls=%async_computation | async-start | bytes 4194304 | tf_op jit(solution)/shard_map/all_to_all | solution.py:71
  177.7 17.7 %all-to-all-done = bf16[4,128,2048]{2,1,0:T(8,128)(2,1)} async-done(((bf16[4,128,2048]{2,1,0:T(8,128)(2,1)}), bf16[4,128,2048]{2,1,0:T(8,128)(2,1)}, u32[]{:S(2)}, u32[]{:S(2)}) %all-to-all-start) | async-done | bytes 2097184 | tf_op jit(solution)/shard_map/all_to_all | solution.py:71
  195.4 2.1 convert_reduce_fusion.1
  199.3 19.8 %all_to_all.15 = bf16[4,128,2048]{2,1,0:T(8,128)(2,1)} all-to-all(bf16[4,128,2048]{2,1,0:T(8,128)(2,1)S(1)} %broadcast_in_dim.39), channel_id=1, replica_groups=mesh['sp_0'=8,'sp_1'=4,'sp_2'=2,'tp'=4] {'tp'}, dimensions={0} | all-to-all | bytes 4194304 | tf_op jit(solution)/shard_map/all_to_all | solution.py:77
  219.1 16.5 %fusion.7 = bf16[512,2048]{1,0:T(8,128)(2,1)} fusion(bf16[2048,4096]{1,0:T(8,128)(2,1)} %all-gather.8.cloned.1.call-done, bf16[512,2048]{1,0:T(8,128)(2,1)} %bitcast.138), kind=kOutput, calls=%fused_computation.14 | convolution fusion | flops 8594128896 | bytes 20971520 | tf_op jit(solution)/shard_map/dot_general | solution.py:193
  235.5 20.1 %all_to_all.16 = bf16[4,128,2048]{2,1,0:T(8,128)(2,1)S(1)} all-to-all(bf16[4,128,2048]{2,1,0:T(8,128)(2,1)} %bitcast.139), channel_id=1, replica_groups=mesh['sp_0'=8,'sp_1'=4,'sp_2'=2,'tp'=4] {'tp'}, dimensions={0} | all-to-all | bytes 4194304 | tf_op jit(solution)/shard_map/all_to_all | solution.py:71
  (173 shorter events, 22.7 us)
Async XLA Ops:
  6.5 164.1 %copy-start = (bf16[512,2048]{1,0:T(8,128)(2,1)S(1)}, bf16[512,2048]{1,0:T(8,128)(2,1)}, u32[]{:S(2)}) copy-start(bf16[512,2048]{1,0:T(8,128)(2,1)} %param.22) | copy-start | bytes 6291460
  6.5 212.5 %all-gather.8.cloned.1.call-start = ((), (), s32[]{:S(2)}) async-start(), calls=%async_computation.3 | async-start | bytes 17039360 | tf_op jit(solution)/shard_map/all_gather | solution.py:16
  9.3 8.4 %collective-permute-start = (bf16[3,512]{0,1:T(8,128)(2,1)S(1)}, bf16[3,512]{0,1:T(8,128)(2,1)S(1)}, u32[]{:S(2)}, u32[]{:S(2)}) collective-permute-start(bf16[3,512]{0,1:T(8,128)(2,1)S(1)} %copy.31), channel_id=1, source_target_pairs={{0,4},{4,8},{8,12},{12,16},{16,20},{20,24},{24,28},{28,32},{32,36}... | collective-permute-start | bytes 9224 | tf_op jit(solution)/shard_map/ppermute | solution.py:23
  19.0 1.3 copy-start.6
  20.4 0.9 copy-start.7
  21.3 0.7 copy-start.5
  24.6 2.7 %copy-start.1 = (f32[512,512]{0,1:T(8,128)S(1)}, f32[512,512]{0,1:T(8,128)}, u32[]{:S(2)}) copy-start(f32[512,512]{0,1:T(8,128)} %get-tuple-element.110) | copy-start | bytes 3145732
  121.7 47.0 %copy-start.2 = (f32[16,32,512]{2,0,1:T(8,128)S(1)}, f32[16,32,512]{2,0,1:T(8,128)}, u32[]{:S(2)}) copy-start(f32[16,32,512]{2,0,1:T(8,128)} %get-tuple-element.46) | copy-start | bytes 3145732
  126.9 43.3 %copy-start.3 = (bf16[512,512]{1,0:T(8,128)(2,1)S(1)}, bf16[512,512]{1,0:T(8,128)(2,1)}, u32[]{:S(2)}) copy-start(bf16[512,512]{1,0:T(8,128)(2,1)} %param.15) | copy-start | bytes 1572868
  173.2 22.2 %all-to-all-start = ((bf16[4,128,2048]{2,1,0:T(8,128)(2,1)}), bf16[4,128,2048]{2,1,0:T(8,128)(2,1)}, u32[]{:S(2)}, u32[]{:S(2)}) async-start(bf16[4,128,2048]{2,1,0:T(8,128)(2,1)} %bitcast.137), calls=%async_computation | async-start | bytes 4194304 | tf_op jit(solution)/shard_map/all_to_all | solution.py:71
  177.7 21.2 %copy-start.4 = (f32[2048]{0:T(1024)S(1)}, f32[2048]{0:T(1024)}, u32[]{:S(2)}) copy-start(f32[2048]{0:T(1024)} %param.23) | copy-start | bytes 24580
Sparse Core Ops, SparseCore 0:
  10.1 100.2 all-gather.7
where the time goes:
time: 266 us; the launch traced here: 264 us
  local copies, waits for them, and re-layouts  107 us (40%)
  blocking collectives  81.4 us (31%)
  matrix products  20 us (8%)
  waiting for transfers between devices  19.7 us (7%)
  other arithmetic  15.1 us (6%)
  between operations  13.9 us (5%)
  starting transfers between devices  6.38 us (2%)
    dynamic_update_slice x64, local copies, waits for them, and re-layouts, local(): lax.scan(step_rows, start_carry, (keep_blocks, drive_blocks))  70.5 us
    all_gather x3, blocking collectives, gathered_once(): both, at, found = (lax.all_gather(jnp.concatenate(lines), axis), 0, {})  41.6 us
    dynamic_slice x16, local copies, waits for them, and re-layouts, local(): lax.scan(step_rows, start_carry, (keep_blocks, drive_blocks))  21.5 us
    all_to_all x1, blocking collectives, sum_at_owner(): pieces = lax.all_to_all(split_up(value, dim, size), axis, 0, 0, tiled=True)  20.1 us
    all_to_all x1, blocking collectives, copy_for_each(): return lax.all_to_all(copies, axis, split_axis=0, concat_axis=0, tiled=True)  19.8 us
    all_to_all x1, waiting for transfers between devices, sum_at_owner(): pieces = lax.all_to_all(split_up(value, dim, size), axis, 0, 0, tiled=True)  17.7 us
    dot_general x1, matrix products, local(): lax.dot_general(activated, whole_down, (((1,), (1,)), ((), ())), preferre...  16.5 us
    unnamed x20, local copies, waits for them, and re-layouts  6.74 us
  transfers between devices with their start and end apart: 3, of which 2 were waited for; matrix products, arithmetic and copies ran while one was open for 46% of the time, Pallas kernels for 0%

commit v1 on v0

v1 whole, which is shorter than its diff:
```python
import jax
import jax.numpy as jnp
from jax import lax
from jax.experimental import pallas as pl
from jax.experimental.pallas import tpu as pltpu
from jax.sharding import Mesh
from jax.sharding import PartitionSpec as P

MESH = pl.DeviceIdType.MESH
SP = ("z", "x", "c")
SP_TP = ("z", "x", "c", "y")
NZ, NX, NC, NY = 8, 4, 2, 4
ROWS = 512
CH = 512
D = 2048
F = 2048
SEG = 64
HALF = 1024
TILE = 256
N_COPIES = 160
F32 = jnp.float32
BF16 = jnp.bfloat16


class Copies:
    def __init__(self, send, recv):
        self.send, self.recv, self.made = send, recv, []

    def go(self, src, dst, device):
        k = len(self.made)
        assert k < N_COPIES
        copy = pltpu.make_async_remote_copy(
            src_ref=src,
            dst_ref=dst,
            send_sem=self.send.at[k],
            recv_sem=self.recv.at[k],
            device_id=device,
            device_id_type=MESH,
        )
        copy.start()
        self.made.append(copy)
        return copy

    def finish(self):
        for copy in self.made:
            copy.wait_send()


def one_minus_exp(y):
    poly = 1.0 - y * (1.0 / 9.0)
    for k in range(8, 1, -1):
        poly = 1.0 - y * (1.0 / k) * poly
    return y * poly


def kernel(
    residual_hbm,
    gate_hbm,
    value_hbm,
    conv_hbm,
    rate_hbm,
    input_hbm,
    decay_hbm,
    step_hbm,
    out_w_hbm,
    gain_hbm,
    up_hbm,
    down_hbm,
    result_hbm,
    value,
    gate,
    step,
    conv,
    rate_w,
    input_w,
    decay,
    out_w,
    gain,
    residual,
    up_w,
    down_w,
    gate_pair,
    keep,
    drive,
    gelu,
    entry_p,
    entry_s,
    pay,
    plane,
    pay_z,
    column,
    gated,
    mixed,
    normed,
    act,
    part,
    first_l,
    first_r,
    comb_l,
    comb_r,
    from_dn,
    from_up,
    updated,
    result,
    local_sem,
    send_sem,
    recv_sem,
):
    z = lax.axis_index("z")
    x = lax.axis_index("x")
    c = lax.axis_index("c")
    y = lax.axis_index("y")

    loads = {}

    def load(name, src, dst):
        copy = pltpu.make_async_copy(src, dst, local_sem.at[len(loads)])
        copy.start()
        loads[name] = copy

    load("value", value_hbm, value.at[pl.ds(16, ROWS)])
    load("up", up_hbm, up_w.at[z, x, c])
    load("down", down_hbm, down_w.at[z, x, c])
    load("rate", rate_hbm, rate_w)
    load("input", input_hbm, input_w)
    load("conv", conv_hbm, conv)
    load("decay", decay_hbm, decay)
    load("step", step_hbm, step)
    load("gate", gate_hbm, gate)
    load("out_w", out_w_hbm, out_w)
    load("gain", gain_hbm, gain)
    load("residual", residual_hbm.at[pl.ds(pl.multiple_of(y * 128, 128), 128)], residual)

    here = {"z": z, "x": x, "c": c, "y": y}

    def at(**other):
        return {**here, **other}

    line = (z * NX + x) * NC + c

    def on_line(k):
        return at(z=k // (NX * NC), x=(k // NC) % NX, c=k % NC)

    x_up, x_dn = at(x=(x + 1) % NX), at(x=(x + NX - 1) % NX)
    z_up, z_dn = at(z=(z + 1) % NZ), at(z=(z + NZ - 1) % NZ)
    y_up_k, y_dn_k, y_op_k = (y + 1) % NY, (y + NY - 1) % NY, (y + 2) % NY
    y_up, y_dn = at(y=y_up_k), at(y=y_dn_k)
    partner = at(c=1 - c)
    next_row = on_line((line + 1) % (NZ * NX * NC))
    prev_row = on_line((line + NZ * NX * NC - 1) % (NZ * NX * NC))
    plane_peers = [
        at(x=(x + dx) % NX, c=(c + dc) % NC) for dx in range(NX) for dc in range(NC) if dx or dc
    ]
    column_peers = [at(z=(z + dz) % NZ) for dz in range(1, NZ)]
    greeted = [next_row, prev_row, y_up, y_dn, *plane_peers, *column_peers]
    barrier = pltpu.get_barrier_semaphore()
    for device in greeted:
        pl.semaphore_signal(barrier, inc=1, device_id=device, device_id_type=MESH)

    copies = Copies(send_sem, recv_sem)
    go = copies.go

    loads["value"].wait()
    loads["up"].wait()
    loads["down"].wait()
    pl.semaphore_wait(barrier, len(greeted))

    halo = go(value.at[pl.ds(ROWS, 16)], value.at[pl.ds(0, 16)], next_row)

    swaps = []

    def swap(ref):
        swaps.append(go(ref, ref, partner))

    def zz(distance):
        return (z + NZ + distance) % NZ

    def xx(distance):
        return (x + NX + distance) % NX

    own_up = up_w.at[z, x, c]
    own_down = down_w.at[z, x, c]
    up_x = [go(own_up, own_up, x_up), go(own_up, own_up, x_dn)]
    down_z = {(1, 0): go(own_down, own_down, z_up), (1, 1): go(own_down, own_down, z_dn)}
    up_z = {}
    down_x = {}

    def event_up_x1():
        up_x[0].wait_recv()
        ref = up_w.at[z, xx(-1), c, pl.ds(0, 16)]
        up_x.append(go(ref, ref, x_up))
        up_x[1].wait_recv()
        ref = up_w.at[z, xx(1), c, pl.ds(16, 16)]
        up_x.append(go(ref, ref, x_dn))

    def event_up_x2():
        up_x[2].wait_recv()
        up_x[3].wait_recv()
        for h in range(2):
            ref = up_w.at[z, pl.ds(2 * h, 2), c]
            up_z[1, h, 0] = go(ref, ref, z_up)
            up_z[1, h, 1] = go(ref, ref, z_dn)
        swap(up_w.at[z, :, c])

    def event_up_z(d, h):
        def run():
            for way, device, sign in ((0, z_up, -1), (1, z_dn, 1)):
                if (d, h, way) not in up_z:
                    continue
                up_z[d, h, way].wait_recv()
                ref = up_w.at[zz(sign * d), pl.ds(2 * h, 2), c]
                if d < 3 or (d == 3 and h == way):
                    up_z[d + 1, h, way] = go(ref, ref, device)
                swap(ref)

        return run

    def start_down_x(k, zk):
        ref = down_w.at[zk, x, c]
        down_x[k] = [go(ref, ref, x_up), go(ref, ref, x_dn), zk]

    def event_down_z(d):
        def run():
            for way, device, sign in ((0, z_up, -1), (1, z_dn, 1)):
                down_z[d, way].wait_recv()
                source = zz(sign * d)
                if d < 3:
                    ref = down_w.at[source, x, c]
                    down_z[d + 1, way] = go(ref, ref, device)
                elif d == 3:
                    ref = down_w.at[source, x, c, pl.ds(16 * way, 16)]
                    down_z[d + 1, way] = go(ref, ref, device)
                if d < 4:
                    start_down_x(2 * d - 1 + way, source)
            if d == 4:
                start_down_x(7, zz(4))

        return run

    def event_down_x(k):
        def run():
            first, second, zk = down_x[k]
            first.wait_recv()
            if k % 2 == 0:
                ref = down_w.at[zk, xx(-1), c]
                last = go(ref, ref, x_up)
            second.wait_recv()
            if k % 2 == 1:
                ref = down_w.at[zk, xx(1), c]
                last = go(ref, ref, x_dn)
            down_x[k].append(last)

        return run

    def event_down_x2(k):
        def run():
            down_x[k][3].wait_recv()
            swap(down_w.at[down_x[k][2], :, c])

        return run

    start_down_x(0, z)
    events = [
        event_up_x1,
        event_down_z(1),
        event_up_x2,
        event_down_x(0),
        event_down_z(2),
        event_down_x2(0),
        event_down_x(1),
        event_down_z(3),
        event_up_z(1, 0),
        event_down_x2(1),
        event_down_x(2),
        event_down_z(4),
        event_up_z(1, 1),
        event_down_x2(2),
        event_down_x(3),
        event_up_z(2, 0),
        event_down_x2(3),
        event_down_x(4),
        event_up_z(2, 1),
        event_down_x2(4),
        event_down_x(5),
        event_up_z(3, 0),
        event_down_x2(5),
        event_down_x(6),
        event_up_z(3, 1),
        event_down_x2(6),
        event_down_x(7),
        event_down_x2(7),
        event_up_z(4, 0),
        event_up_z(4, 1),
    ]

    def pump(count):
        for _ in range(count):
            if events:
                events.pop(0)()

    loads["rate"].wait()
    loads["input"].wait()
    loads["conv"].wait()
    loads["decay"].wait()
    loads["step"].wait()
    empty = jnp.zeros((64, 64), BF16)
    for g in range(4):
        top = [rate_w[2 * g], empty, input_w[2 * g], empty]
        low = [empty, rate_w[2 * g + 1], empty, input_w[2 * g + 1]]
        gate_pair[g, 0:64, :] = jnp.concatenate(top, axis=1)
        gate_pair[g, 64:128, :] = jnp.concatenate(low, axis=1)

    def gates(block):
        start = pl.multiple_of(block * SEG, SEG)
        for g in range(4):
            lanes = pl.ds(g * 128, 128)
            window = value[pl.ds(start, SEG + 16), lanes].astype(F32)
            filtered = jnp.zeros((SEG, 128), F32)
            for tap in range(4):
                back = 3 - tap
                moved = pltpu.roll(window, back, 0) if back else window
                filtered = filtered + moved[16:] * conv[tap : tap + 1, lanes]
            smoothed = filtered.astype(BF16)
            logits = jnp.dot(smoothed, gate_pair[g], preferred_element_type=F32)
            rate = jax.nn.sigmoid(logits[:, :128])
            admit = jax.nn.sigmoid(logits[:, 128:])
            rows = pl.ds(start, SEG)
            log_keep = -8.0 * step[rows, lanes] * rate * decay[0:1, lanes]
            kept = jnp.exp(log_keep)
            lost = -2.0 * log_keep
            gap = jnp.where(lost < 0.5, one_minus_exp(jnp.minimum(lost, 0.5)), 1.0 - kept * kept)
            keep[g, rows, :] = kept
            drive[g, rows, :] = jnp.sqrt(gap) * admit * smoothed.astype(F32)

    def gates_step(block, carry):
        gates(block)
        return carry

    lax.fori_loop(1, ROWS // SEG, gates_step, 0)
    halo.wait_recv()

    @pl.when(line == 0)
    def _():
        value[0:16, :] = jnp.zeros((16, CH), BF16)

    gates(0)
    pump(1)

    def scan_step(t, carry):
        rows = pl.ds(t, 8, stride=SEG)
        after = []
        for g in range(4):
            product, state = carry[g]
            kept = keep[g, rows, :]
            product = product * kept
            state = kept * state + drive[g, rows, :]
            keep[g, rows, :] = product
            drive[g, rows, :] = state
            after.append((product, state))
        return tuple(after)

    fresh_carry = (jnp.ones((8, 128), F32), jnp.zeros((8, 128), F32))
    ends = lax.fori_loop(0, SEG, scan_step, (fresh_carry,) * 4, unroll=4)
    for g in range(4):
        product, state = ends[g]
        total_p, total_s = jnp.ones((1, 128), F32), jnp.zeros((1, 128), F32)
        for s in range(8):
            entry_p[g, s : s + 1, :] = total_p
            entry_s[g, s : s + 1, :] = total_s
            total_s = product[s : s + 1] * total_s + state[s : s + 1]
            total_p = total_p * product[s : s + 1]
        pay[g : g + 1, :] = total_p
        pay[g + 4 : g + 5, :] = total_s

    own_plane = x * NC + c
    plane[own_plane] = pay[...]
    in_plane = [go(pay, plane.at[own_plane], device) for device in plane_peers]
    pump(2)
    loads["gate"].wait()

    def gelu_step(block, carry):
        rows = pl.ds(pl.multiple_of(block * SEG, SEG), SEG)
        gelu[rows, :] = jax.nn.gelu(gate[rows, :].astype(F32), approximate=True)
        return carry

    lax.fori_loop(0, ROWS // SEG, gelu_step, 0)
    for copy in in_plane:
        copy.wait_recv()

    def prefix(pieces, size, index):
        run_p, run_s = jnp.ones((4, 128), F32), jnp.zeros((4, 128), F32)
        before_p, before_s = run_p, run_s
        for k in range(size):
            before_p = jnp.where(k == index, run_p, before_p)
            before_s = jnp.where(k == index, run_s, before_s)
            piece = pieces[k]
            run_s = piece[0:4] * run_s + piece[4:8]
            run_p = run_p * piece[0:4]
        return before_p, before_s, run_p, run_s

    inside_p, inside_s, run_p, run_s = prefix(plane, NX * NC, own_plane)
    pay_z[0:4, :] = run_p
    pay_z[4:8, :] = run_s
    column[z] = pay_z[...]
    in_column = [go(pay_z, column.at[z], device) for device in column_peers]
    pump(1)
    for copy in in_column:
        copy.wait_recv()
    _, outer_s, _, _ = prefix(column, NZ, z)
    carried = inside_p * outer_s + inside_s
    for g in range(4):
        entry_s[g] = entry_s[g] + entry_p[g] * carried[g : g + 1]

    for s in range(8):
        rows = pl.ds(s * SEG, SEG)
        for g in range(4):
            lanes = pl.ds(g * 128, 128)
            hidden = drive[g, rows, :] + keep[g, rows, :] * entry_s[g, s : s + 1, :]
            gated[s % 2, s // 2, :, lanes] = (gelu[rows, lanes] * hidden).astype(BF16)

    left, right = pl.ds(0, HALF), pl.ds(HALF, HALF)

    def scatter_start(pieces, slot):
        return {
            "l1": go(pieces.at[y_op_k, :, left], first_l.at[slot], y_dn),
            "r1": go(pieces.at[y_op_k, :, right], first_r.at[slot], y_up),
            "l0": go(pieces.at[y_up_k, :, left], from_dn.at[slot, :, left], y_up),
            "r0": go(pieces.at[y_dn_k, :, right], from_up.at[slot, :, right], y_dn),
        }

    def scatter_pass(pieces, slot, ring):
        ring["l1"].wait_recv()
        comb_l[slot] = (
            pieces[y_dn_k, :, left].astype(F32) + first_l[slot].astype(F32)
        ).astype(BF16)
        ring["l2"] = go(comb_l.at[slot], from_up.at[slot, :, left], y_dn)
        ring["r1"].wait_recv()
        comb_r[slot] = (
            pieces[y_up_k, :, right].astype(F32) + first_r[slot].astype(F32)
        ).astype(BF16)
        ring["r2"] = go(comb_r.at[slot], from_dn.at[slot, :, right], y_up)

    def scatter_end(pieces, slot, ring):
        for name in ("l0", "r0", "l2", "r2"):
            ring[name].wait_recv()
        return (
            pieces[y].astype(F32) + from_dn[slot].astype(F32) + from_up[slot].astype(F32)
        )

    def gather_start(rows):
        l, r = rows.at[y, :, left], rows.at[y, :, right]
        return [go(l, l, y_up), go(r, r, y_dn), go(r, r, y_up), go(l, l, y_dn)]

    def gather_pass(rows, ring):
        ring[0].wait_recv()
        ref = rows.at[y_dn_k, :, left]
        ring.append(go(ref, ref, y_up))
        ring[1].wait_recv()
        ref = rows.at[y_up_k, :, right]
        ring.append(go(ref, ref, y_dn))

    def gather_end(ring):
        for copy in ring[2:]:
            copy.wait_recv()

    loads["out_w"].wait()

    def project(q):
        rows = gated[q].reshape(4 * SEG, CH)

        def tile_step(n, carry):
            cols = pl.ds(pl.multiple_of(n * TILE, TILE), TILE)
            tile = jnp.dot(rows, out_w[:, cols], preferred_element_type=F32).astype(BF16)
            mixed[q, :, :, cols] = tile.reshape(4, SEG, TILE)
            return carry

        lax.fori_loop(0, D // TILE, tile_step, 0)

    def settle(q, ring):
        total = scatter_end(mixed.at[q], q, ring)
        fresh = (residual[pl.ds(q * SEG, SEG), :].astype(F32) + total).astype(BF16)
        updated[pl.ds(q * SEG, SEG), :] = fresh
        wide = fresh.astype(F32)
        factor = lax.rsqrt(jnp.mean(wide * wide, axis=-1, keepdims=True) + 1e-06)
        normed[q, y] = (wide * factor * gain[...]).astype(BF16)

    loads["residual"].wait()
    loads["gain"].wait()
    project(0)
    ring0 = scatter_start(mixed.at[0], 0)
    project(1)
    pump(2)
    scatter_pass(mixed.at[0], 0, ring0)
    ring1 = scatter_start(mixed.at[1], 1)
    pump(6)
    settle(0, ring0)
    gather0 = gather_start(normed.at[0])
    scatter_pass(mixed.at[1], 1, ring1)
    pump(6)
    gather_pass(normed.at[0], gather0)
    settle(1, ring1)
    gather1 = gather_start(normed.at[1])
    pump(6)
    gather_end(gather0)
    gather_pass(normed.at[1], gather1)
    pump(100)
    for copy in swaps:
        copy.wait_recv()

    def feed(q):
        rows = normed[q].reshape(4 * SEG, D)

        def up_step(n, carry):
            cols = pl.ds(pl.multiple_of(n * TILE, TILE), TILE)
            weight = up_w[:, :, :, :, cols].reshape(D, TILE)
            lifted = jnp.maximum(jnp.dot(rows, weight, preferred_element_type=F32), 0.0)
            act[:, cols] = (lifted * lifted).astype(BF16)
            return carry

        lax.fori_loop(0, F // TILE, up_step, 0)
        lhs = act[...]

        def down_step(n, carry):
            cols = pl.ds(pl.multiple_of(n * TILE, TILE), TILE)
            weight = down_w[n].reshape(TILE, F)
            tile = lax.dot_general(
                lhs, weight, (((1,), (1,)), ((), ())), preferred_element_type=F32
            )
            part[q, :, :, cols] = tile.astype(BF16).reshape(4, SEG, TILE)
            return carry

        lax.fori_loop(0, D // TILE, down_step, 0)

    def close(q, ring):
        total = scatter_end(part.at[q], 2 + q, ring)
        rows = pl.ds(q * SEG, SEG)
        result[rows, :] = (updated[rows, :].astype(F32) + total).astype(BF16)

    feed(0)
    ring2 = scatter_start(part.at[0], 2)
    gather_end(gather1)
    feed(1)
    scatter_pass(part.at[0], 2, ring2)
    ring3 = scatter_start(part.at[1], 3)
    close(0, ring2)
    scatter_pass(part.at[1], 3, ring3)
    close(1, ring3)
    store = pltpu.make_async_copy(result, result_hbm, local_sem.at[len(loads)])
    store.start()
    copies.finish()
    store.wait()


def local(
    residual_in,
    gate_in,
    value_in,
    conv_weight,
    rate_weight,
    input_weight,
    decay_base,
    step_scale,
    out_weight,
    norm_gain,
    up_weight,
    down_weight,
):
    vmem = pltpu.VMEM
    scratch = [
        vmem((ROWS + 16, CH), BF16),
        vmem((ROWS, CH), BF16),
        vmem((ROWS, CH), F32),
        vmem((4, CH), F32),
        vmem((8, 64, 64), BF16),
        vmem((8, 64, 64), BF16),
        vmem((1, CH), F32),
        vmem((CH, D), BF16),
        vmem((1, D), F32),
        vmem((128, D), BF16),
        vmem((NZ, NX, NC, 32, F), BF16),
        vmem((NZ, NX, NC, 32, F), BF16),
        vmem((4, 128, 256), BF16),
        vmem((4, ROWS, 128), F32),
        vmem((4, ROWS, 128), F32),
        vmem((ROWS, CH), F32),
        vmem((4, 8, 128), F32),
        vmem((4, 8, 128), F32),
        vmem((8, 128), F32),
        vmem((NX * NC, 8, 128), F32),
        vmem((8, 128), F32),
        vmem((NZ, 8, 128), F32),
        vmem((2, 4, SEG, CH), BF16),
        vmem((2, 4, SEG, D), BF16),
        vmem((2, 4, SEG, D), BF16),
        vmem((4 * SEG, F), BF16),
        vmem((2, 4, SEG, D), BF16),
        vmem((4, SEG, HALF), BF16),
        vmem((4, SEG, HALF), BF16),
        vmem((4, SEG, HALF), BF16),
        vmem((4, SEG, HALF), BF16),
        vmem((4, SEG, D), BF16),
        vmem((4, SEG, D), BF16),
        vmem((128, D), BF16),
        vmem((128, D), BF16),
        pltpu.SemaphoreType.DMA((16,)),
        pltpu.SemaphoreType.DMA((N_COPIES,)),
        pltpu.SemaphoreType.DMA((N_COPIES,)),
    ]
    return pl.pallas_call(
        kernel,
        out_shape=jax.ShapeDtypeStruct((128, D), BF16),
        in_specs=[pl.BlockSpec(memory_space=pl.ANY)] * 12,
        out_specs=pl.BlockSpec(memory_space=pl.ANY),
        scratch_shapes=scratch,
        compiler_params=pltpu.CompilerParams(
            collective_id=0, has_side_effects=True, vmem_limit_bytes=62 * 1024 * 1024
        ),
    )(
        residual_in,
        gate_in,
        value_in,
        conv_weight,
        rate_weight,
        input_weight,
        decay_base.reshape(1, -1),
        step_scale,
        out_weight,
        norm_gain.reshape(1, -1),
        up_weight,
        down_weight,
    )


def solution(mesh):
    split = Mesh(mesh.devices.reshape(NZ, NX, NC, NY), ("z", "x", "c", "y"))
    return jax.shard_map(
        local,
        mesh=split,
        in_specs=(
            P(SP, None),
            P(SP, "y"),
            P(SP, "y"),
            P(None, "y"),
            P("y", None, None),
            P("y", None, None),
            P("y"),
            P(SP, "y"),
            P("y", None),
            P(),
            P(SP, "y"),
            P(SP, "y"),
        ),
        out_specs=P(SP_TP, None),
        check_vma=False,
    )
```

time: 266 us -> 113 us (0.42)
  the two profiles are of different devices: /device:TPU:64 before, /device:TPU:1 now
where the time goes in v1:
time: 113 us
  Pallas kernels  111 us (98%)
  local copies, waits for them, and re-layouts  1.88 us (2%)
    pallas_call x1, Pallas kernels, local(): pl.pallas_call(kernel, out_shape=jax.ShapeDtypeStruct((128, D), BF16), in...  111 us

profile of v1, /device:TPU:1, one launch (start us, length us, event | category | flops | bytes accessed | tf_op | source)
XLA Modules:
  0.0 113.4 jit_solution(835614207641336220)
XLA Ops:
  0.0 111.5 %shard_map.118 = bf16[128,2048]{1,0:T(8,128)(2,1)} custom-call(bf16[512,2048]{1,0:T(8,128)(2,1)} %residual_hbm.1, bf16[512,512]{1,0:T(8,128)(2,1)} %gate_hbm.1, bf16[512,512]{1,0:T(8,128)(2,1)} %value_hbm.1, f32[4,512]{1,0:T(4,128)} %conv_hbm.1, bf16[8,64,64]{2,1,0:T(8,128)(2,1)} %rate_hbm.1, bf16[8,64,64]{2,1,0:T(8,128)(2,1)} %input_hbm.1, ...), custom_call_target="tpu_custom_call" | custom-call | tf_op jit(solution)/shard_map/pallas_call | solution.py:609
  111.5 1.9 %copy.14 = bf16[128,2048]{1,0:T(8,128)(2,1)} copy(bf16[128,2048]{1,0:T(8,128)(2,1)} %shard_map.118) | data formatting | bytes 1048576

commit v2 on v1

--- a/solution.py
+++ b/solution.py
@@ -7,6 +7,7 @@
 from jax.sharding import PartitionSpec as P
 
 MESH = pl.DeviceIdType.MESH
+scope = jax.named_scope
 SP = ("z", "x", "c")
 SP_TP = ("z", "x", "c", "y")
 NZ, NX, NC, NY = 8, 4, 2, 4
@@ -15,8 +16,9 @@
 D = 2048
 F = 2048
 SEG = 64
+PITCH = SEG + 8
 HALF = 1024
-TILE = 256
+TILE = 512
 N_COPIES = 160
 F32 = jnp.float32
 BF16 = jnp.bfloat16
@@ -161,9 +163,53 @@
     go = copies.go
 
     loads["value"].wait()
-    loads["up"].wait()
-    loads["down"].wait()
-    pl.semaphore_wait(barrier, len(greeted))
+    loads["rate"].wait()
+    loads["input"].wait()
+    loads["conv"].wait()
+    loads["decay"].wait()
+    loads["step"].wait()
+    empty = jnp.zeros((64, 64), BF16)
+    for g in range(4):
+        top = [rate_w[2 * g], empty, input_w[2 * g], empty]
+        low = [empty, rate_w[2 * g + 1], empty, input_w[2 * g + 1]]
+        gate_pair[g, 0:64, :] = jnp.concatenate(top, axis=1)
+        gate_pair[g, 64:128, :] = jnp.concatenate(low, axis=1)
+
+    def gates(block):
+        start = pl.multiple_of(block * SEG, SEG)
+        for g in range(4):
+            lanes = pl.ds(g * 128, 128)
+            window = value[pl.ds(start, SEG + 16), lanes].astype(F32)
+            filtered = jnp.zeros((SEG, 128), F32)
+            for tap in range(4):
+                back = 3 - tap
+                moved = pltpu.roll(window, back, 0) if back else window
+                filtered = filtered + moved[16:] * conv[tap : tap + 1, lanes]
+            smoothed = filtered.astype(BF16)
+            logits = jnp.dot(smoothed, gate_pair[g], preferred_element_type=F32)
+            rate = jax.nn.sigmoid(logits[:, :128])
+            admit = jax.nn.sigmoid(logits[:, 128:])
+            rows = pl.ds(start, SEG)
+            log_keep = -8.0 * step[rows, lanes] * rate * decay[0:1, lanes]
+            kept = jnp.exp(log_keep)
+            lost = -2.0 * log_keep
+            gap = jnp.where(lost < 0.5, one_minus_exp(jnp.minimum(lost, 0.5)), 1.0 - kept * kept)
+            spread = pl.ds(pl.multiple_of(block * PITCH, 8), SEG)
+            keep[g, spread, :] = kept
+            drive[g, spread, :] = jnp.sqrt(gap) * admit * smoothed.astype(F32)
+
+    def gates_step(block, carry):
+        gates(block)
+        return carry
+
+    with scope("gates"):
+        lax.fori_loop(1, ROWS // SEG, gates_step, 0)
+
+    with scope("load_wait"):
+        loads["up"].wait()
+        loads["down"].wait()
+    with scope("barrier"):
+        pl.semaphore_wait(barrier, len(greeted))
 
     halo = go(value.at[pl.ds(ROWS, 16)], value.at[pl.ds(0, 16)], next_row)
 
@@ -259,13 +305,13 @@
 
         return run
 
-    start_down_x(0, z)
     events = [
         event_up_x1,
+        lambda: start_down_x(0, z),
         event_down_z(1),
         event_up_x2,
+        event_down_z(2),
         event_down_x(0),
-        event_down_z(2),
         event_down_x2(0),
         event_down_x(1),
         event_down_z(3),
@@ -293,61 +339,25 @@
         event_up_z(4, 1),
     ]
 
+    total_events = len(events)
+
     def pump(count):
         for _ in range(count):
             if events:
-                events.pop(0)()
-
-    loads["rate"].wait()
-    loads["input"].wait()
-    loads["conv"].wait()
-    loads["decay"].wait()
-    loads["step"].wait()
-    empty = jnp.zeros((64, 64), BF16)
-    for g in range(4):
-        top = [rate_w[2 * g], empty, input_w[2 * g], empty]
-        low = [empty, rate_w[2 * g + 1], empty, input_w[2 * g + 1]]
-        gate_pair[g, 0:64, :] = jnp.concatenate(top, axis=1)
-        gate_pair[g, 64:128, :] = jnp.concatenate(low, axis=1)
-
-    def gates(block):
-        start = pl.multiple_of(block * SEG, SEG)
-        for g in range(4):
-            lanes = pl.ds(g * 128, 128)
-            window = value[pl.ds(start, SEG + 16), lanes].astype(F32)
-            filtered = jnp.zeros((SEG, 128), F32)
-            for tap in range(4):
-                back = 3 - tap
-                moved = pltpu.roll(window, back, 0) if back else window
-                filtered = filtered + moved[16:] * conv[tap : tap + 1, lanes]
-            smoothed = filtered.astype(BF16)
-            logits = jnp.dot(smoothed, gate_pair[g], preferred_element_type=F32)
-            rate = jax.nn.sigmoid(logits[:, :128])
-            admit = jax.nn.sigmoid(logits[:, 128:])
-            rows = pl.ds(start, SEG)
-            log_keep = -8.0 * step[rows, lanes] * rate * decay[0:1, lanes]
-            kept = jnp.exp(log_keep)
-            lost = -2.0 * log_keep
-            gap = jnp.where(lost < 0.5, one_minus_exp(jnp.minimum(lost, 0.5)), 1.0 - kept * kept)
-            keep[g, rows, :] = kept
-            drive[g, rows, :] = jnp.sqrt(gap) * admit * smoothed.astype(F32)
-
-    def gates_step(block, carry):
-        gates(block)
-        return carry
-
-    lax.fori_loop(1, ROWS // SEG, gates_step, 0)
-    halo.wait_recv()
+                with scope(f"event_{total_events - len(events)}"):
+                    events.pop(0)()
+
+    with scope("halo"):
+        halo.wait_recv()
 
     @pl.when(line == 0)
     def _():
         value[0:16, :] = jnp.zeros((16, CH), BF16)
 
     gates(0)
-    pump(1)
 
     def scan_step(t, carry):
-        rows = pl.ds(t, 8, stride=SEG)
+        rows = pl.ds(t, 8, stride=PITCH)
         after = []
         for g in range(4):
             product, state = carry[g]
@@ -360,7 +370,8 @@
         return tuple(after)
 
     fresh_carry = (jnp.ones((8, 128), F32), jnp.zeros((8, 128), F32))
-    ends = lax.fori_loop(0, SEG, scan_step, (fresh_carry,) * 4, unroll=4)
+    with scope("scan"):
+        ends = lax.fori_loop(0, SEG, scan_step, (fresh_carry,) * 4, unroll=4)
     for g in range(4):
         product, state = ends[g]
         total_p, total_s = jnp.ones((1, 128), F32), jnp.zeros((1, 128), F32)
@@ -375,7 +386,7 @@
     own_plane = x * NC + c
     plane[own_plane] = pay[...]
     in_plane = [go(pay, plane.at[own_plane], device) for device in plane_peers]
-    pump(2)
+    pump(3)
     loads["gate"].wait()
 
     def gelu_step(block, carry):
@@ -383,9 +394,11 @@
         gelu[rows, :] = jax.nn.gelu(gate[rows, :].astype(F32), approximate=True)
         return carry
 
-    lax.fori_loop(0, ROWS // SEG, gelu_step, 0)
-    for copy in in_plane:
-        copy.wait_recv()
+    with scope("gelu"):
+        lax.fori_loop(0, ROWS // SEG, gelu_step, 0)
+    with scope("plane"):
+        for copy in in_plane:
+            copy.wait_recv()
 
     def prefix(pieces, size, index):
         run_p, run_s = jnp.ones((4, 128), F32), jnp.zeros((4, 128), F32)
@@ -403,9 +416,10 @@
     pay_z[4:8, :] = run_s
     column[z] = pay_z[...]
     in_column = [go(pay_z, column.at[z], device) for device in column_peers]
-    pump(1)
-    for copy in in_column:
-        copy.wait_recv()
+    pump(3)
+    with scope("column"):
+        for copy in in_column:
+            copy.wait_recv()
     _, outer_s, _, _ = prefix(column, NZ, z)
     carried = inside_p * outer_s + inside_s
     for g in range(4):
@@ -415,7 +429,8 @@
         rows = pl.ds(s * SEG, SEG)
         for g in range(4):
             lanes = pl.ds(g * 128, 128)
-            hidden = drive[g, rows, :] + keep[g, rows, :] * entry_s[g, s : s + 1, :]
+            spread = pl.ds(s * PITCH, SEG)
+            hidden = drive[g, spread, :] + keep[g, spread, :] * entry_s[g, s : s + 1, :]
             gated[s % 2, s // 2, :, lanes] = (gelu[rows, lanes] * hidden).astype(BF16)
 
     left, right = pl.ds(0, HALF), pl.ds(HALF, HALF)
@@ -486,26 +501,31 @@
 
     loads["residual"].wait()
     loads["gain"].wait()
-    project(0)
+    def phase(name, call, *args):
+        with scope(name):
+            return call(*args)
+
+    phase("project0", project, 0)
     ring0 = scatter_start(mixed.at[0], 0)
-    project(1)
+    phase("project1", project, 1)
     pump(2)
-    scatter_pass(mixed.at[0], 0, ring0)
+    phase("pass0", scatter_pass, mixed.at[0], 0, ring0)
     ring1 = scatter_start(mixed.at[1], 1)
     pump(6)
-    settle(0, ring0)
+    phase("settle0", settle, 0, ring0)
     gather0 = gather_start(normed.at[0])
-    scatter_pass(mixed.at[1], 1, ring1)
+    phase("pass1", scatter_pass, mixed.at[1], 1, ring1)
     pump(6)
-    gather_pass(normed.at[0], gather0)
-    settle(1, ring1)
+    phase("gpass0", gather_pass, normed.at[0], gather0)
+    phase("settle1", settle, 1, ring1)
     gather1 = gather_start(normed.at[1])
     pump(6)
-    gather_end(gather0)
-    gather_pass(normed.at[1], gather1)
+    phase("gend0", gather_end, gather0)
+    phase("gpass1", gather_pass, normed.at[1], gather1)
     pump(100)
-    for copy in swaps:
-        copy.wait_recv()
+    with scope("swaps"):
+        for copy in swaps:
+            copy.wait_recv()
 
     def feed(q):
         rows = normed[q].reshape(4 * SEG, D)
@@ -522,7 +542,7 @@
 
         def down_step(n, carry):
             cols = pl.ds(pl.multiple_of(n * TILE, TILE), TILE)
-            weight = down_w[n].reshape(TILE, F)
+            weight = down_w[pl.ds(2 * n, 2)].reshape(TILE, F)
             tile = lax.dot_general(
                 lhs, weight, (((1,), (1,)), ((), ())), preferred_element_type=F32
             )
@@ -536,19 +556,20 @@
         rows = pl.ds(q * SEG, SEG)
         result[rows, :] = (updated[rows, :].astype(F32) + total).astype(BF16)
 
-    feed(0)
+    phase("feed0", feed, 0)
     ring2 = scatter_start(part.at[0], 2)
-    gather_end(gather1)
-    feed(1)
-    scatter_pass(part.at[0], 2, ring2)
+    phase("gend1", gather_end, gather1)
+    phase("feed1", feed, 1)
+    phase("pass2", scatter_pass, part.at[0], 2, ring2)
     ring3 = scatter_start(part.at[1], 3)
-    close(0, ring2)
-    scatter_pass(part.at[1], 3, ring3)
-    close(1, ring3)
+    phase("close0", close, 0, ring2)
+    phase("pass3", scatter_pass, part.at[1], 3, ring3)
+    phase("close1", close, 1, ring3)
     store = pltpu.make_async_copy(result, result_hbm, local_sem.at[len(loads)])
     store.start()
-    copies.finish()
-    store.wait()
+    with scope("finish"):
+        copies.finish()
+        store.wait()
 
 
 def local(
@@ -580,8 +601,8 @@
         vmem((NZ, NX, NC, 32, F), BF16),
         vmem((NZ, NX, NC, 32, F), BF16),
         vmem((4, 128, 256), BF16),
-        vmem((4, ROWS, 128), F32),
-        vmem((4, ROWS, 128), F32),
+        vmem((4, 8 * PITCH, 128), F32),
+        vmem((4, 8 * PITCH, 128), F32),
         vmem((ROWS, CH), F32),
         vmem((4, 8, 128), F32),
         vmem((4, 8, 128), F32),

time: 113 us -> 101 us (0.89)
  Pallas kernels: 111 us -> 98.6 us
    pallas_call x1, Pallas kernels: 111 us -> 98.6 us  [local(): pl.pallas_call(kernel, out_shape=jax.ShapeDtypeStruct((128, D), BF16), in...]
where the time goes in v2:
time: 101 us
  Pallas kernels  98.6 us (98%)
  local copies, waits for them, and re-layouts  1.88 us (2%)
    pallas_call x1, Pallas kernels, local(): pl.pallas_call(kernel, out_shape=jax.ShapeDtypeStruct((128, D), BF16), in...  98.6 us

profile of v2, /device:TPU:1, one launch (start us, length us, event | category | flops | bytes accessed | tf_op | source)
XLA Modules:
  0.0 100.5 jit_solution(11826795014273885269)
XLA Ops:
  0.0 98.6 %shard_map.118 = bf16[128,2048]{1,0:T(8,128)(2,1)} custom-call(bf16[512,2048]{1,0:T(8,128)(2,1)} %residual_hbm.1, bf16[512,512]{1,0:T(8,128)(2,1)} %gate_hbm.1, bf16[512,512]{1,0:T(8,128)(2,1)} %value_hbm.1, f32[4,512]{1,0:T(4,128)} %conv_hbm.1, bf16[8,64,64]{2,1,0:T(8,128)(2,1)} %rate_hbm.1, bf16[8,64,64]{2,1,0:T(8,128)(2,1)} %input_hbm.1, ...), custom_call_target="tpu_custom_call" | custom-call | tf_op jit(solution)/shard_map/pallas_call | solution.py:630
  98.6 1.9 %copy.14 = bf16[128,2048]{1,0:T(8,128)(2,1)} copy(bf16[128,2048]{1,0:T(8,128)(2,1)} %shard_map.118) | data formatting | bytes 1048576
